TPU v7x, 32 devices: a whole 2x2x4 slice. The times are simulated.
32 devices in a mesh: fs: 4 (over y, x), tp: 8 (over z, core).
Axes of the slice: x: 2, y: 2, z: 4, core: 2. Of those that a mesh axis runs over, the one named last changes fastest.
Arguments:
- tokens: bfloat16 [4096, 2048], P(('fs', 'tp')), may hold values from -6 to 6
- up_weight: bfloat16 [2048, 4096], P('fs', 'tp'), may hold values from -0.125 to 0.125
- down_weight: bfloat16 [4096, 2048], P('tp', 'fs'), may hold values from -0.09375 to 0.09375
- cotangent: bfloat16 [4096, 2048], P(('fs', 'tp')), may hold values from -6 to 6
Outputs:
- input_grad: bfloat16 [4096, 2048], P(('fs', 'tp'))
- up_grad: float32 [2048, 4096], P('fs', 'tp')
- down_grad: float32 [4096, 2048], P('tp', 'fs')
All inputs are finite; a program needn't handle non-finite values.
Results may differ from a plain program's by a relative error of at most 0.018.
Values may be sent and summed in bfloat16 or wider, within the bound.
A program may use at most 128 MiB of HBM per device.

v0:
```python
import jax
import jax.numpy as jnp
from jax import lax
from jax.sharding import PartitionSpec as P


def shards(tokens, up_weight, down_weight, cotangent):
    rows_all, cot_all = (
        lax.all_gather(tokens, "tp", axis=0, tiled=True),
        lax.all_gather(cotangent, "tp", axis=0, tiled=True),
    )
    up_whole = lax.all_gather(up_weight, "fs", axis=0, tiled=True)
    pre = jnp.dot(rows_all, up_whole, preferred_element_type=jnp.float32)
    active = jnp.maximum(pre, 0.0)
    hidden = (active * active).astype(jnp.bfloat16)
    part = cot_all
    dhidden = lax.dot_general(
        part,
        lax.all_gather(down_weight, "fs", axis=1, tiled=True),
        (((1,), (1,)), ((), ())),
        preferred_element_type=jnp.float32,
    )
    dpre = (2.0 * active * dhidden).astype(jnp.bfloat16)
    count_all = tokens.shape[0] * lax.axis_size("fs") * lax.axis_size("tp")
    factor = 1.0 / jnp.sqrt(jnp.float32(count_all))
    part = rows_all
    up_grad = (
        lax.psum_scatter(
            lax.dot_general(
                part, dpre, (((0,), (0,)), ((), ())), preferred_element_type=jnp.float32
            ).astype(jnp.bfloat16),
            "fs",
            scatter_dimension=0,
            tiled=True,
        ).astype(jnp.float32)
        * factor
    )
    down_term = lax.dot_general(
        hidden, cot_all, (((0,), (0,)), ((), ())), preferred_element_type=jnp.float32
    )
    down_grad = (
        lax.psum_scatter(
            down_term.astype(jnp.bfloat16), "fs", scatter_dimension=1, tiled=True
        ).astype(jnp.float32)
        * factor
    )
    part = dpre
    prod = lax.dot_general(
        part, up_whole, (((1,), (1,)), ((), ())), preferred_element_type=jnp.float32
    )
    rounded = lax.optimization_barrier(prod.astype(jnp.bfloat16))
    grad_rows = lax.psum_scatter(
        rounded.astype(jnp.float32).astype(jnp.bfloat16), "tp", scatter_dimension=0, tiled=True
    )
    return (grad_rows, up_grad, down_grad)


def solution(mesh):
    placed = (P(("fs", "tp"), None), P("fs", "tp"), P("tp", "fs"), P(("fs", "tp"), None))
    return jax.shard_map(
        shards,
        mesh=mesh,
        in_specs=placed,
        out_specs=(P(("fs", "tp"), None), P("fs", "tp"), P("tp", "fs")),
        check_vma=False,
    )
```

profile of v0, /device:TPU:0, one launch (start us, length us, event | category | flops | bytes accessed | tf_op | source)
XLA Modules:
  0.0 314.8 jit_solution(16396900336464673650)
XLA Ops:
  7.2 0.0 all-gather.7.cloned.1.call-start
  7.2 0.7 all-gather.7.cloned.1.call-update
  7.9 0.0 all-gather.5.cloned.1.call-start
  7.9 0.7 all-gather.5.cloned.1.call-update
  8.6 0.0 all-gather.9.cloned.1.call-start
  8.7 0.7 all-gather.9.cloned.1.call-update
  9.4 0.0 all-gather.11.cloned.1.call-start
  9.4 0.5 all-gather.11.cloned.1.call-update
  10.0 0.0 reduce-scatter.8.cloned.1.call-start
  10.0 37.7 %all-gather.7.cloned.1.call-done = bf16[2048,512]{1,0:T(8,128)(2,1)} async-done(((bf16[512,512]{1,0:T(8,128)(2,1)}), bf16[2048,512]{1,0:T(8,128)(2,1)}) %all-gather.7.cloned.1.call-update) | async-done | bytes 2097168 | tf_op jit(solution)/shard_map/all_gather | solution.py:12
  47.8 48.5 %all-gather.5.cloned.1.call-done = bf16[1024,2048]{1,0:T(8,128)(2,1)} async-done(((bf16[128,2048]{1,0:T(8,128)(2,1)}), bf16[1024,2048]{1,0:T(8,128)(2,1)}) %all-gather.5.cloned.1.call-update) | async-done | bytes 4194320 | tf_op jit(solution)/shard_map/all_gather | solution.py:9
  96.2 5.2 %fusion.3 = f32[1024,512]{1,0:T(8,128)S(1)} fusion(bf16[1024,2048]{1,0:T(8,128)(2,1)} %all-gather.5.cloned.1.call-done, bf16[2048,512]{1,0:T(8,128)(2,1)} %all-gather.7.cloned.1.call-done), kind=kOutput, calls=%fused_computation.10 | convolution fusion | flops 2147483648 | bytes 8388608 | tf_op jit(solution)/shard_map/dot_general | solution.py:13
  101.4 42.1 %all-gather.9.cloned.1.call-done = bf16[1024,2048]{1,0:T(8,128)(2,1)} async-done(((bf16[128,2048]{1,0:T(8,128)(2,1)}), bf16[1024,2048]{1,0:T(8,128)(2,1)}) %all-gather.9.cloned.1.call-update) | async-done | bytes 4194320 | tf_op jit(solution)/shard_map/all_gather | solution.py:10
  143.6 5.9 %convolution_convert_fusion.1 = bf16[512,2048]{0,1:T(8,128)(2,1)} fusion(bf16[1024,2048]{1,0:T(8,128)(2,1)} %all-gather.9.cloned.1.call-done, f32[1024,512]{1,0:T(8,128)S(1)} %fusion.3), kind=kOutput, calls=%fused_computation.1 | convolution fusion | flops 2150105088 | bytes 8388608 | tf_op jit(solution)/shard_map/dot_general | solution.py:38
  149.5 0.0 reduce-scatter.8.cloned.1.call-update
  149.5 0.0 reduce-scatter.6.cloned.1.call-start
  149.5 29.6 %all-gather.11.cloned.1.call-done = bf16[512,2048]{1,0:T(8,128)(2,1)} async-done(((bf16[512,512]{1,0:T(8,128)(2,1)}), bf16[512,2048]{1,0:T(8,128)(2,1)}) %all-gather.11.cloned.1.call-update) | async-done | bytes 2097168 | tf_op jit(solution)/shard_map/all_gather | solution.py:19
  179.1 0.0 copy-start
  179.1 5.4 %multiply_convert_fusion.1 = bf16[1024,512]{1,0:T(8,128)(2,1)S(1)} fusion(f32[1024,512]{1,0:T(8,128)S(1)} %fusion.3, bf16[1024,2048]{1,0:T(8,128)(2,1)} %all-gather.9.cloned.1.call-done, bf16[512,2048]{1,0:T(8,128)(2,1)} %all-gather.11.cloned.1.call-done), kind=kOutput, calls=%fused_computation.5 | convolution fusion | flops 2149580800 | bytes 9437184 | tf_op jit(solution)/shard_map/dot_general | solution.py:17
  184.5 0.0 copy-done
  184.5 3.7 %fusion = bf16[2048,512]{0,1:T(8,128)(2,1)} fusion(bf16[1024,512]{1,0:T(8,128)(2,1)S(1)} %multiply_convert_fusion.1, bf16[1024,2048]{1,0:T(8,128)(2,1)S(1)} %copy-done), kind=kOutput, calls=%fused_computation.3 | convolution fusion | flops 2148532224 | bytes 7340032 | tf_op jit(solution)/shard_map/dot_general | solution.py:29
  188.2 0.0 copy-start.1
  188.2 0.0 reduce-scatter.6.cloned.1.call-update
  188.2 0.0 reduce-scatter.4.cloned.1.call-start
  188.3 1.6 copy-done.1
  189.9 4.3 %convolution_convert_fusion = bf16[1024,2048]{1,0:T(8,128)(2,1)} fusion(bf16[1024,512]{1,0:T(8,128)(2,1)S(1)} %multiply_convert_fusion.1, bf16[2048,512]{1,0:T(8,128)(2,1)S(1)} %copy-done.1), kind=kOutput, calls=%fused_computation | convolution fusion | flops 2149580800 | bytes 7340032 | tf_op jit(solution)/shard_map/dot_general | solution.py:48
  194.2 0.0 reduce-scatter.4.cloned.1.call-update
  194.2 23.0 %reduce-scatter.8.cloned.1.call-done = bf16[512,512]{0,1:T(8,128)(2,1)} async-done(((bf16[512,2048]{0,1:T(8,128)(2,1)}), bf16[512,512]{0,1:T(8,128)(2,1)}) %reduce-scatter.8.cloned.1.call-update) | async-done | bytes 524304 | tf_op jit(solution)/shard_map/reduce_scatter | solution.py:42
  217.1 1.2 convert_multiply_fusion
  218.3 1.3 copy.9
  219.6 35.5 %reduce-scatter.6.cloned.1.call-done = bf16[512,512]{0,1:T(8,128)(2,1)} async-done(((bf16[2048,512]{0,1:T(8,128)(2,1)}), bf16[512,512]{0,1:T(8,128)(2,1)}) %reduce-scatter.6.cloned.1.call-update) | async-done | bytes 524304 | tf_op jit(solution)/shard_map/reduce_scatter | solution.py:28
  255.2 1.2 convert_multiply_fusion.1
  256.4 1.3 copy.8
  257.7 50.3 %reduce-scatter.4.cloned.1.call-done = bf16[128,2048]{1,0:T(8,128)(2,1)} async-done(((bf16[1024,2048]{1,0:T(8,128)(2,1)}), bf16[128,2048]{1,0:T(8,128)(2,1)}) %reduce-scatter.4.cloned.1.call-update) | async-done | bytes 524304 | tf_op jit(solution)/shard_map/reduce_scatter | solution.py:52
Async XLA Ops:
  7.2 40.6 %all-gather.7.cloned.1.call-start = ((), (), s32[]{:S(2)}) async-start(), calls=%async_computation.4 | async-start | bytes 2621440 | tf_op jit(solution)/shard_map/all_gather | solution.py:12
  7.9 88.3 %all-gather.5.cloned.1.call-start = ((), (), s32[]{:S(2)}) async-start(), calls=%async_computation.3 | async-start | bytes 4718592 | tf_op jit(solution)/shard_map/all_gather | solution.py:9
  8.6 134.9 %all-gather.9.cloned.1.call-start = ((), (), s32[]{:S(2)}) async-start(), calls=%async_computation.5 | async-start | bytes 4718592 | tf_op jit(solution)/shard_map/all_gather | solution.py:10
  9.4 169.7 %all-gather.11.cloned.1.call-start = ((), (), s32[]{:S(2)}) async-start(), calls=%async_computation.6 | async-start | bytes 2621440 | tf_op jit(solution)/shard_map/all_gather | solution.py:19
  10.0 207.2 %reduce-scatter.8.cloned.1.call-start = ((), (), s32[]{:S(2)}) async-start(), calls=%async_computation.9 | async-start | bytes 2621440 | tf_op jit(solution)/shard_map/reduce_scatter | solution.py:42
  149.5 105.7 %reduce-scatter.6.cloned.1.call-start = ((), (), s32[]{:S(2)}) async-start(), calls=%async_computation.8 | async-start | bytes 2621440 | tf_op jit(solution)/shard_map/reduce_scatter | solution.py:28
  179.1 5.4 %copy-start = (bf16[1024,2048]{1,0:T(8,128)(2,1)S(1)}, bf16[1024,2048]{1,0:T(8,128)(2,1)}, u32[]{:S(2)}) copy-start(bf16[1024,2048]{1,0:T(8,128)(2,1)} %all-gather.5.cloned.1.call-done) | copy-start | bytes 12582916
  188.2 1.6 copy-start.1
  188.2 119.7 %reduce-scatter.4.cloned.1.call-start = ((), (), s32[]{:S(2)}) async-start(), calls=%async_computation.7 | async-start | bytes 4718592 | tf_op jit(solution)/shard_map/reduce_scatter | solution.py:52
Sparse Core Ops, SparseCore 0:
  9.8 37.8 all-gather.6
  49.3 46.8 all-gather.4
  97.8 45.6 all-gather.8
  145.2 33.8 all-gather.10
  181.9 35.1 reduce-scatter.7
  220.0 35.1 reduce-scatter.5
  258.0 49.8 reduce-scatter.3
where the time goes:
time: 315 us
  waiting for transfers between devices  269 us (85%)
  matrix products  24.5 us (8%)
  between operations  14.2 us (5%)
  local copies, waits for them, and re-layouts  4.18 us (1%)
    reduce_scatter x1, waiting for transfers between devices, shards(): lax.psum_scatter(rounded.astype(jnp.float32).astype(jnp.bfloat16), 'tp',...  50.3 us
    all_gather x1, waiting for transfers between devices, shards(): lax.all_gather(tokens, 'tp', axis=0, tiled=True)  48.5 us
    all_gather x1, waiting for transfers between devices, shards(): lax.all_gather(cotangent, 'tp', axis=0, tiled=True)  42.1 us
    all_gather x1, waiting for transfers between devices, shards(): up_whole = lax.all_gather(up_weight, 'fs', axis=0, tiled=True)  37.7 us
    reduce_scatter x1, waiting for transfers between devices, shards(): lax.psum_scatter(lax.dot_general(part, dpre, (((0,), (0,)), ((), ())), pr...  35.5 us
    all_gather x1, waiting for transfers between devices, shards(): lax.all_gather(down_weight, 'fs', axis=1, tiled=True)  29.6 us
    reduce_scatter x1, waiting for transfers between devices, shards(): lax.psum_scatter(down_term.astype(jnp.bfloat16), 'fs', scatter_dimension=...  23 us
  transfers between devices with their start and end apart: 7, of which 7 were waited for; matrix products, arithmetic and copies ran while one was open for 9% of the time, Pallas kernels for 0%

commit v1 on v0

v1 whole, which is shorter than its diff:
```python
import functools

import jax
import jax.numpy as jnp
from jax import lax
from jax.experimental import pallas as pl
from jax.experimental.pallas import tpu as pltpu
from jax.sharding import PartitionSpec as P

MESH = pl.DeviceIdType.MESH
BF16 = jnp.bfloat16
F32 = jnp.float32


def ring_index(p):
    q, b = p // 2, p % 2
    return 2 * q + b + (q % 2) * (1 - 2 * b)


def dot(a, b, ca, cb):
    return lax.dot_general(a, b, (((ca,), (cb,)), ((), ())), preferred_element_type=F32)


def kernel(
    nfs, nz, factor,
    tok_in, up_in, down_in, cot_in,
    dx_out, ug_out, dg_out,
    tok, cot, up, down, hid, dpre,
    dx_own, dx_send, dx_recv, dr_send, dr_recv,
    ug_own, dg_own, ug_send, ug_recv, dg_send, dg_recv,
    local_sem, zs, zr, ps, pr, ws, wr, gs, gr, xs, xr, rs, rr,
):
    fs, tp = lax.axis_index("fs"), lax.axis_index("tp")
    rows, width = tok_in.shape
    h = rows // 2
    block = 4 * h
    dl = up_in.shape[0]
    fl = up_in.shape[1]
    z, core = tp // 2, tp % 2
    pos = ring_index(fs)
    fwd = (fs, ((z + 1) % nz) * 2 + core)
    bwd = (fs, ((z + nz - 1) % nz) * 2 + core)
    mate = (fs, 2 * z + 1 - core)
    cw = (ring_index((pos + 1) % nfs), tp)
    ccw = (ring_index((pos + nfs - 1) % nfs), tp)

    def cols(o):
        return pl.ds(pl.multiple_of(o * dl, dl), dl)

    locals_ = [
        pltpu.make_async_copy(tok_in, tok.at[pl.ds(0, rows)], local_sem.at[0]),
        pltpu.make_async_copy(up_in, up.at[cols(fs)], local_sem.at[1]),
        pltpu.make_async_copy(down_in, down.at[:, cols(fs)], local_sem.at[2]),
        pltpu.make_async_copy(cot_in, cot.at[pl.ds(0, rows)], local_sem.at[3]),
    ]
    for c in locals_:
        c.start()
    barrier = pltpu.get_barrier_semaphore()
    peers = (fwd, bwd, mate, cw, ccw)
    for peer in peers:
        pl.semaphore_signal(barrier, inc=1, device_id=peer, device_id_type=MESH)
    pl.semaphore_wait(barrier, len(peers))
    for c in locals_:
        c.wait()

    sends = []

    def remote(src, dst, s, r, peer):
        c = pltpu.make_async_remote_copy(
            src_ref=src, dst_ref=dst, send_sem=s, recv_sem=r, device_id=peer, device_id_type=MESH
        )
        c.start()
        sends.append(c)
        return c

    bufs = (tok, cot)

    def z_send(k, a):
        out = []
        for d, peer in enumerate((fwd, bwd)):
            out.append(remote(
                bufs[a].at[pl.ds(k * block + d * h, h)],
                bufs[a].at[pl.ds((k + 1) * block + d * h, h)],
                zs.at[k, d, a], zr.at[k, d, a], peer,
            ))
        return out

    def mate_send(k, a):
        return remote(
            bufs[a].at[pl.ds(k * block, 2 * h)],
            bufs[a].at[pl.ds(k * block + 2 * h, 2 * h)],
            ps.at[k, a], pr.at[k, a], mate,
        )

    def w_send(k, half):
        a = ring_index((pos + nfs - k) % nfs)
        b = ring_index((pos + k) % nfs)
        n = dl // 2
        piece = up.at[pl.ds(pl.multiple_of(a * dl + half * n, n), n)]
        m = fl // 2
        other = down.at[pl.ds(half * m, m), cols(b)]
        return [
            remote(piece, piece, ws.at[k, half, 0], wr.at[k, half, 0], cw),
            remote(other, other, ws.at[k, half, 1], wr.at[k, half, 1], ccw),
        ]

    z_copy, w_copy, mate_copy = {}, {}, {}
    for a in range(2):
        z_copy[0, a] = z_send(0, a)
        w_copy[0, a] = w_send(0, a)
    for a in range(2):
        mate_copy[0, a] = mate_send(0, a)

    def hidden_block(s):
        here = pl.ds(s * block, block)
        active = jnp.maximum(dot(tok[here, :], up[...], 1, 0), 0.0)
        hid[here, :] = (active * active).astype(BF16)
        dh = dot(cot[here, :], down[...], 1, 1)
        dpre[here, :] = (2.0 * active * dh).astype(BF16)

    pair_copy = {}

    def dx_block(s):
        here = pl.ds(s * block, block)

        def tile(j, carry):
            c = cols(j)
            part = dot(dpre[here, :], up[c, :], 1, 1)
            dx_own[s, :, c] = part[: 2 * h]
            dx_send[s, :, c] = part[2 * h :].astype(BF16)
            return carry

        lax.fori_loop(0, nfs, tile, 0)
        pair_copy[s] = remote(dx_send.at[s], dx_recv.at[s], xs.at[s], xr.at[s], mate)

    events = []
    for k in range(nfs - 1):
        for half in range(2):
            events.append(((2 * k + half + 1) * 1.5 / (nfs - 1), 1, k, half))
    for k in range(nz - 1):
        for a in range(2):
            events.append(((2 * k + a + 1) * 3.0 / (nz - 1), 0, k, a))
    events.sort()
    weights_left = 2 * (nfs - 1)
    ready = [0]

    def settle(s):
        for a in range(2):
            mate_copy[s, a].wait_recv()
        hidden_block(s)
        if s < nz - 1:
            dx_block(s)

    for _, kind, k, a in events:
        if kind == 1:
            for c in w_copy[k, a]:
                c.wait_recv()
            if k + 1 < nfs - 1:
                w_copy[k + 1, a] = w_send(k + 1, a)
            weights_left -= 1
        else:
            for c in z_copy[k, a]:
                c.wait_recv()
            if k + 1 < nz - 1:
                z_copy[k + 1, a] = z_send(k + 1, a)
            mate_copy[k + 1, a] = mate_send(k + 1, a)
            if a == 1:
                ready.append(k + 1)
        if weights_left == 0:
            for s in ready:
                settle(s)
            ready = []
    for s in ready:
        settle(s)

    def up_term(r):
        o = ring_index((pos + nfs - r - 1) % nfs)
        return dot(tok[:, cols(o)], dpre[...], 0, 0)

    def down_term(r):
        o = ring_index((pos + r + 1) % nfs)
        return dot(hid[...], cot[:, cols(o)], 0, 0)

    g_copy = {}

    def g_send(r, half):
        n, m = dl // 2, fl // 2
        a, b = pl.ds(half * n, n), pl.ds(half * m, m)
        g_copy[r, half] = [
            remote(ug_send.at[r, a], ug_recv.at[r, a], gs.at[r, half, 0], gr.at[r, half, 0], cw),
            remote(dg_send.at[r, b], dg_recv.at[r, b], gs.at[r, half, 1], gr.at[r, half, 1], ccw),
        ]

    def g_first():
        ug_send[0] = up_term(0).astype(BF16)
        dg_send[0] = down_term(0).astype(BF16)
        for half in range(2):
            g_send(0, half)
        ug_own[...] = up_term(1)
        dg_own[...] = down_term(1)

    def g_step(r):
        n, m = dl // 2, fl // 2
        for half in range(2):
            for c in g_copy[r - 1, half]:
                c.wait_recv()
            a, b = pl.ds(half * n, n), pl.ds(half * m, m)
            gu = ug_own[a, :] + ug_recv[r - 1, a, :].astype(F32)
            gd = dg_own[b, :] + dg_recv[r - 1, b, :].astype(F32)
            if r < nfs - 1:
                ug_send[r, a, :] = gu.astype(BF16)
                dg_send[r, b, :] = gd.astype(BF16)
                g_send(r, half)
            else:
                ug_out[a, :] = gu * factor
                dg_out[b, :] = gd * factor
        if r < nfs - 1:
            ug_own[...] = up_term(r + 1)
            dg_own[...] = down_term(r + 1)

    x_copy = {}

    def x_step(r):
        s = r + 1 if r < nz - 1 else 0
        pair_copy[s].wait_recv()
        for d, peer in enumerate((fwd, bwd)):
            here = pl.ds(d * h, h)
            if r > 0:
                x_copy[r - 1, d].wait_recv()
            total = dx_own[s, here, :] + dx_recv[s, here, :].astype(F32)
            if r > 0:
                total = total + dr_recv[r - 1, here, :].astype(F32)
            if r < nz - 1:
                dr_send[r, here, :] = total.astype(BF16)
                x_copy[r, d] = remote(
                    dr_send.at[r, here], dr_recv.at[r, here], rs.at[r, d], rr.at[r, d], peer
                )
            else:
                dx_out[here, :] = total.astype(BF16)

    g_first()
    x_step(0)
    dx_block(nz - 1)
    for r in range(1, max(nfs, nz)):
        if r < nfs:
            g_step(r)
        if r < nz:
            x_step(r)
    for c in sends:
        c.wait_send()


def shards(nfs, ntp, tokens, up_weight, down_weight, cotangent):
    rows, width = tokens.shape
    dl, fl = up_weight.shape
    nz = ntp // 2
    whole = rows * ntp
    factor = 1.0 / (whole * nfs) ** 0.5
    dma = pltpu.SemaphoreType.DMA
    any_space = pl.BlockSpec(memory_space=pl.ANY)
    vmem = pl.BlockSpec(memory_space=pltpu.VMEM)
    return pl.pallas_call(
        functools.partial(kernel, nfs, nz, factor),
        out_shape=(
            jax.ShapeDtypeStruct((rows, width), BF16),
            jax.ShapeDtypeStruct((dl, fl), F32),
            jax.ShapeDtypeStruct((fl, dl), F32),
        ),
        in_specs=[any_space] * 4,
        out_specs=(vmem, vmem, vmem),
        scratch_shapes=[
            pltpu.VMEM((whole, width), BF16),
            pltpu.VMEM((whole, width), BF16),
            pltpu.VMEM((width, fl), BF16),
            pltpu.VMEM((fl, width), BF16),
            pltpu.VMEM((whole, fl), BF16),
            pltpu.VMEM((whole, fl), BF16),
            pltpu.VMEM((nz, rows, width), F32),
            pltpu.VMEM((nz, rows, width), BF16),
            pltpu.VMEM((nz, rows, width), BF16),
            pltpu.VMEM((nz - 1, rows, width), BF16),
            pltpu.VMEM((nz - 1, rows, width), BF16),
            pltpu.VMEM((dl, fl), F32),
            pltpu.VMEM((fl, dl), F32),
            pltpu.VMEM((nfs - 1, dl, fl), BF16),
            pltpu.VMEM((nfs - 1, dl, fl), BF16),
            pltpu.VMEM((nfs - 1, fl, dl), BF16),
            pltpu.VMEM((nfs - 1, fl, dl), BF16),
            dma((4,)),
            dma((nz - 1, 2, 2)), dma((nz - 1, 2, 2)),
            dma((nz, 2)), dma((nz, 2)),
            dma((nfs - 1, 2, 2)), dma((nfs - 1, 2, 2)),
            dma((nfs - 1, 2, 2)), dma((nfs - 1, 2, 2)),
            dma((nz,)), dma((nz,)),
            dma((nz - 1, 2)), dma((nz - 1, 2)),
        ],
        compiler_params=pltpu.CompilerParams(
            collective_id=0, has_side_effects=True, vmem_limit_bytes=67_000_000
        ),
    )(tokens, up_weight, down_weight, cotangent)


def solution(mesh):
    placed = (P(("fs", "tp"), None), P("fs", "tp"), P("tp", "fs"), P(("fs", "tp"), None))
    return jax.shard_map(
        functools.partial(shards, mesh.shape["fs"], mesh.shape["tp"]),
        mesh=mesh,
        in_specs=placed,
        out_specs=(P(("fs", "tp"), None), P("fs", "tp"), P("tp", "fs")),
        check_vma=False,
    )
```

time: 315 us -> 127 us (0.40)
  waiting for transfers between devices: 269 us -> 0 us
  Pallas kernels: 0 us -> 121 us
  matrix products: 24.5 us -> 0 us
  between operations: 14.2 us -> 0.65 us
    all_gather x4 -> x0, waiting for transfers between devices: 158 us -> none  [the longest x1 48.5 us: shards(): lax.all_gather(tokens, 'tp', axis=0, tiled=True)]
    pallas_call x0 -> x1, Pallas kernels: none -> 121 us  [shards(): pl.pallas_call(functools.partial(kernel, nfs, nz, factor), out_shape=(jax...]
    reduce_scatter x3 -> x0, waiting for transfers between devices: 109 us -> none  [the longest x1 50.3 us: shards(): lax.psum_scatter(rounded.astype(jnp.float32).astype(jnp.bfloat16), 'tp',...]
    dot_general x5 -> x0, matrix products: 24.5 us -> none  [the longest x1 5.91 us: shards(): lax.dot_general(hidden, cot_all, (((0,), (0,)), ((), ())), preferred_elem...]
  transfers between devices with their start and end apart: 7 -> 0, of which waited for: 7 -> 0; matrix products, arithmetic and copies ran while one was open for 9% -> 0% of each run, Pallas kernels for 0% -> 0%
where the time goes in v1:
time: 127 us
  Pallas kernels  121 us (95%)
  local copies, waits for them, and re-layouts  4.55 us (4%)
    pallas_call x1, Pallas kernels, shards(): pl.pallas_call(functools.partial(kernel, nfs, nz, factor), out_shape=(jax...  121 us
    unnamed x7, local copies, waits for them, and re-layouts  4.55 us

profile of v1, /device:TPU:0, one launch (start us, length us, event | category | flops | bytes accessed | tf_op | source)
XLA Modules:
  0.0 126.7 jit_solution(10313406709641151406)
XLA Ops:
  0.6 121.5 %shard_map.67 = (bf16[128,2048]{1,0:T(8,128)(2,1)}, f32[512,512]{1,0:T(8,128)}, f32[512,512]{1,0:T(8,128)}) custom-call(bf16[128,2048]{1,0:T(8,128)(2,1)} %tok_in.1, bf16[512,512]{1,0:T(8,128)(2,1)} %up_in.1, bf16[512,512]{1,0:T(8,128)(2,1)} %down_in.1, bf16[128,2048]{1,0:T(8,128)(2,1)} %cot_in.1), custom_call_target="tpu_custom_call" | custom-call | tf_op jit(solution)/shard_map/pallas_call | solution.py:262
  122.1 0.0 copy-start.1
  122.1 2.0 %copy.10 = bf16[128,2048]{1,0:T(8,128)(2,1)} copy(bf16[128,2048]{1,0:T(8,128)(2,1)} %get-tuple-element.6) | data formatting | bytes 1048576
  124.1 0.0 copy-done.1
  124.1 0.0 copy-start
  124.1 1.0 copy.11
  125.1 0.6 copy-done
  125.7 1.0 copy.12
Async XLA Ops:
  122.1 2.0 %copy-start.1 = (f32[512,512]{1,0:T(8,128)S(1)}, f32[512,512]{1,0:T(8,128)}, u32[]{:S(2)}) copy-start(f32[512,512]{1,0:T(8,128)} %get-tuple-element.7) | copy-start | bytes 3145732
  124.1 1.6 %copy-start = (f32[512,512]{1,0:T(8,128)S(1)}, f32[512,512]{1,0:T(8,128)}, u32[]{:S(2)}) copy-start(f32[512,512]{1,0:T(8,128)} %get-tuple-element.8) | copy-start | bytes 3145732

commit v2 on v1

--- a/solution.py
+++ b/solution.py
@@ -133,91 +133,6 @@
         lax.fori_loop(0, nfs, tile, 0)
         pair_copy[s] = remote(dx_send.at[s], dx_recv.at[s], xs.at[s], xr.at[s], mate)
 
-    events = []
-    for k in range(nfs - 1):
-        for half in range(2):
-            events.append(((2 * k + half + 1) * 1.5 / (nfs - 1), 1, k, half))
-    for k in range(nz - 1):
-        for a in range(2):
-            events.append(((2 * k + a + 1) * 3.0 / (nz - 1), 0, k, a))
-    events.sort()
-    weights_left = 2 * (nfs - 1)
-    ready = [0]
-
-    def settle(s):
-        for a in range(2):
-            mate_copy[s, a].wait_recv()
-        hidden_block(s)
-        if s < nz - 1:
-            dx_block(s)
-
-    for _, kind, k, a in events:
-        if kind == 1:
-            for c in w_copy[k, a]:
-                c.wait_recv()
-            if k + 1 < nfs - 1:
-                w_copy[k + 1, a] = w_send(k + 1, a)
-            weights_left -= 1
-        else:
-            for c in z_copy[k, a]:
-                c.wait_recv()
-            if k + 1 < nz - 1:
-                z_copy[k + 1, a] = z_send(k + 1, a)
-            mate_copy[k + 1, a] = mate_send(k + 1, a)
-            if a == 1:
-                ready.append(k + 1)
-        if weights_left == 0:
-            for s in ready:
-                settle(s)
-            ready = []
-    for s in ready:
-        settle(s)
-
-    def up_term(r):
-        o = ring_index((pos + nfs - r - 1) % nfs)
-        return dot(tok[:, cols(o)], dpre[...], 0, 0)
-
-    def down_term(r):
-        o = ring_index((pos + r + 1) % nfs)
-        return dot(hid[...], cot[:, cols(o)], 0, 0)
-
-    g_copy = {}
-
-    def g_send(r, half):
-        n, m = dl // 2, fl // 2
-        a, b = pl.ds(half * n, n), pl.ds(half * m, m)
-        g_copy[r, half] = [
-            remote(ug_send.at[r, a], ug_recv.at[r, a], gs.at[r, half, 0], gr.at[r, half, 0], cw),
-            remote(dg_send.at[r, b], dg_recv.at[r, b], gs.at[r, half, 1], gr.at[r, half, 1], ccw),
-        ]
-
-    def g_first():
-        ug_send[0] = up_term(0).astype(BF16)
-        dg_send[0] = down_term(0).astype(BF16)
-        for half in range(2):
-            g_send(0, half)
-        ug_own[...] = up_term(1)
-        dg_own[...] = down_term(1)
-
-    def g_step(r):
-        n, m = dl // 2, fl // 2
-        for half in range(2):
-            for c in g_copy[r - 1, half]:
-                c.wait_recv()
-            a, b = pl.ds(half * n, n), pl.ds(half * m, m)
-            gu = ug_own[a, :] + ug_recv[r - 1, a, :].astype(F32)
-            gd = dg_own[b, :] + dg_recv[r - 1, b, :].astype(F32)
-            if r < nfs - 1:
-                ug_send[r, a, :] = gu.astype(BF16)
-                dg_send[r, b, :] = gd.astype(BF16)
-                g_send(r, half)
-            else:
-                ug_out[a, :] = gu * factor
-                dg_out[b, :] = gd * factor
-        if r < nfs - 1:
-            ug_own[...] = up_term(r + 1)
-            dg_own[...] = down_term(r + 1)
-
     x_copy = {}
 
     def x_step(r):
@@ -238,14 +153,112 @@
             else:
                 dx_out[here, :] = total.astype(BF16)
 
+    events = []
+    for k in range(nfs - 1):
+        for half in range(2):
+            events.append(((2 * k + half + 1) * 1.5 / (nfs - 1), 1, k, half))
+    for k in range(nz - 1):
+        for a in range(2):
+            events.append(((2 * k + a + 1) * 3.0 / (nz - 1), 0, k, a))
+    events.sort()
+    weights_left = 2 * (nfs - 1)
+    ready = [0]
+
+    def settle(s):
+        for a in range(2):
+            mate_copy[s, a].wait_recv()
+        hidden_block(s)
+        if s < nz - 1:
+            dx_block(s)
+
+    for _, kind, k, a in events:
+        if kind == 1:
+            for c in w_copy[k, a]:
+                c.wait_recv()
+            if k + 1 < nfs - 1:
+                w_copy[k + 1, a] = w_send(k + 1, a)
+            weights_left -= 1
+        else:
+            for c in z_copy[k, a]:
+                c.wait_recv()
+            if k + 1 < nz - 1:
+                z_copy[k + 1, a] = z_send(k + 1, a)
+            mate_copy[k + 1, a] = mate_send(k + 1, a)
+            if a == 1:
+                ready.append(k + 1)
+        if weights_left == 0 and (kind, k) != (0, nz - 2):
+            for s in ready:
+                settle(s)
+            ready = []
+    for s in ready[:-1]:
+        settle(s)
+    x_step(0)
+    settle(ready[-1])
+
+    def up_term(r):
+        o = ring_index((pos + nfs - r - 1) % nfs)
+        return dot(tok[:, cols(o)], dpre[...], 0, 0)
+
+    def down_term(r):
+        o = ring_index((pos + r + 1) % nfs)
+        return dot(hid[...], cot[:, cols(o)], 0, 0)
+
+    g_copy = {}
+
+    def g_send(r, half, which):
+        n, m = dl // 2, fl // 2
+        a, b = pl.ds(half * n, n), pl.ds(half * m, m)
+        if which == 0:
+            g_copy[r, half, 0] = remote(
+                ug_send.at[r, a], ug_recv.at[r, a], gs.at[r, half, 0], gr.at[r, half, 0], cw
+            )
+        else:
+            g_copy[r, half, 1] = remote(
+                dg_send.at[r, b], dg_recv.at[r, b], gs.at[r, half, 1], gr.at[r, half, 1], ccw
+            )
+
+    def g_terms(r):
+        ug_own[...] = up_term(r)
+        dg_own[...] = down_term(r)
+
+    def g_first():
+        ug_send[0] = up_term(0).astype(BF16)
+        for half in range(2):
+            g_send(0, half, 0)
+        dg_send[0] = down_term(0).astype(BF16)
+        for half in range(2):
+            g_send(0, half, 1)
+        g_terms(1)
+
+    def g_step(r, half):
+        n, m = dl // 2, fl // 2
+        a, b = pl.ds(half * n, n), pl.ds(half * m, m)
+        g_copy[r - 1, half, 0].wait_recv()
+        gu = ug_own[a, :] + ug_recv[r - 1, a, :].astype(F32)
+        if r < nfs - 1:
+            ug_send[r, a, :] = gu.astype(BF16)
+            g_send(r, half, 0)
+        else:
+            ug_out[a, :] = gu * factor
+        g_copy[r - 1, half, 1].wait_recv()
+        gd = dg_own[b, :] + dg_recv[r - 1, b, :].astype(F32)
+        if r < nfs - 1:
+            dg_send[r, b, :] = gd.astype(BF16)
+            g_send(r, half, 1)
+        else:
+            dg_out[b, :] = gd * factor
+
     g_first()
-    x_step(0)
     dx_block(nz - 1)
     for r in range(1, max(nfs, nz)):
         if r < nfs:
-            g_step(r)
+            g_step(r, 0)
         if r < nz:
             x_step(r)
+        if r < nfs:
+            g_step(r, 1)
+            if r < nfs - 1:
+                g_terms(r + 1)
     for c in sends:
         c.wait_send()
 

time: 127 us -> 120 us (0.945)
  Pallas kernels: 121 us -> 115 us
    pallas_call x1, Pallas kernels: 121 us -> 115 us  [shards(): pl.pallas_call(functools.partial(kernel, nfs, nz, factor), out_shape=(jax...]
where the time goes in v2:
time: 120 us
  Pallas kernels  115 us (96%)
  local copies, waits for them, and re-layouts  4.55 us (4%)
    pallas_call x1, Pallas kernels, shards(): pl.pallas_call(functools.partial(kernel, nfs, nz, factor), out_shape=(jax...  115 us
    unnamed x7, local copies, waits for them, and re-layouts  4.55 us

profile of v2, /device:TPU:0, one launch (start us, length us, event | category | flops | bytes accessed | tf_op | source)
XLA Modules:
  0.0 119.9 jit_solution(12453583964212716785)
XLA Ops:
  0.6 114.7 %shard_map.67 = (bf16[128,2048]{1,0:T(8,128)(2,1)}, f32[512,512]{1,0:T(8,128)}, f32[512,512]{1,0:T(8,128)}) custom-call(bf16[128,2048]{1,0:T(8,128)(2,1)} %tok_in.1, bf16[512,512]{1,0:T(8,128)(2,1)} %up_in.1, bf16[512,512]{1,0:T(8,128)(2,1)} %down_in.1, bf16[128,2048]{1,0:T(8,128)(2,1)} %cot_in.1), custom_call_target="tpu_custom_call" | custom-call | tf_op jit(solution)/shard_map/pallas_call | solution.py:275
  115.4 0.0 copy-start.1
  115.4 2.0 %copy.10 = bf16[128,2048]{1,0:T(8,128)(2,1)} copy(bf16[128,2048]{1,0:T(8,128)(2,1)} %get-tuple-element.6) | data formatting | bytes 1048576
  117.4 0.0 copy-done.1
  117.4 0.0 copy-start
  117.4 1.0 copy.11
  118.3 0.6 copy-done
  119.0 1.0 copy.12
Async XLA Ops:
  115.4 2.0 %copy-start.1 = (f32[512,512]{1,0:T(8,128)S(1)}, f32[512,512]{1,0:T(8,128)}, u32[]{:S(2)}) copy-start(f32[512,512]{1,0:T(8,128)} %get-tuple-element.7) | copy-start | bytes 3145732
  117.4 1.6 %copy-start = (f32[512,512]{1,0:T(8,128)S(1)}, f32[512,512]{1,0:T(8,128)}, u32[]{:S(2)}) copy-start(f32[512,512]{1,0:T(8,128)} %get-tuple-element.8) | copy-start | bytes 3145732
